TPU v7x, 32 devices: a whole 2x2x4 slice. The times are simulated.
32 devices in a mesh: grp: 2 (over x), sp: 4 (over y, core), tp: 4 (over z).
Axes of the slice: x: 2, y: 2, z: 4, core: 2. Of those that a mesh axis runs over, the one named last changes fastest.
Arguments:
- attention_queryset: bfloat16 [2048, 1024], P(('grp', 'sp'), 'tp'), parts along dimension 0, may hold values from -6 to 6
- attention_keyset: bfloat16 [2048, 1024], P(('grp', 'sp'), 'tp'), parts along dimension 0, may hold values from -6 to 6
- attention_valueset: bfloat16 [2048, 1024], P(('grp', 'sp'), 'tp'), parts along dimension 0, may hold values from -6 to 6
- readout_switch_preactivation: bfloat16 [2048, 1024], P(('grp', 'sp'), 'tp'), parts along dimension 0, may hold values from -6 to 6
- retention_prelinear_score: float32 [2048, 8], P(('grp', 'sp'), 'tp'), parts along dimension 0, may hold values from -6 to 6
- additional_attenuation: float32 [2048, 8], P(('grp', 'sp'), 'tp'), parts along dimension 0, may hold values from -1.9 to 0
- feature_retention_logscale: float32 [8], P('tp'), may hold values from -14 to -2.4
- strength_prelinear_score: float32 [2048, 8], P(('grp', 'sp'), 'tp'), parts along dimension 0, may hold values from -9 to 1
- channel_rescale_vector: bfloat16 [128], replicated, may hold values from 0.099609375 to 1.8984375
- final_projection_matrix: bfloat16 [1024, 2048], replicated, may hold values from -0.1875 to 0.1875
- skip_stream: bfloat16 [2048, 2048], P(('grp', 'sp', 'tp')), parts along dimension 0, may hold values from -6 to 6
- specialist_rescale_vector: bfloat16 [2048], replicated, may hold values from 0.099609375 to 1.8984375
- specialist_switch_matrix: bfloat16 [16, 2048, 512], P(('sp', 'tp')), may hold values from -0.125 to 0.125
- specialist_widen_matrix: bfloat16 [16, 2048, 512], P(('sp', 'tp')), may hold values from -0.125 to 0.125
- specialist_contract_matrix: bfloat16 [16, 512, 2048], P(('sp', 'tp')), may hold values from -0.25 to 0.25
- chosen_specialist_ids: int32 [2048, 4], P(('grp', 'sp', 'tp')), parts along dimension 0, may hold values from 0 to 15, all different within a row; in each aligned block of 64 rows (0 to 63, 64 to 127, ...) at most 32 rows name the same one
- dispatch_shares: float32 [2048, 4], P(('grp', 'sp', 'tp')), parts along dimension 0, may hold values from 0.2 to 1.2
Outputs:
- output: bfloat16 [2048, 2048], P(('grp', 'sp', 'tp')), parts along dimension 0
There are 2 independent parts, one for each index of `grp`. A program takes and returns all parts, laid end to end along the dimension named above; an argument that names none is the same for every part. Nothing has to cross between parts.
Inputs may be any that keep to these rules, and one draw needn't show every extreme that they name: `chosen_specialist_ids`: each row names 4 different experts; among the rows of one device no expert is named more than 32 times, a bound that some block reaches.
All inputs are finite; a program needn't handle non-finite values.
Results may differ from a plain program's by a relative error of at most 0.018.
Values may be sent and summed in bfloat16 or wider, within the bound.
A program may use at most 64 MiB of HBM per device.

v0:
```python
import jax
import jax.numpy as jnp
from jax import lax
from jax.sharding import PartitionSpec as P

HK = 128
BLK = 64


epsilon = 1e-06
exact_mode = lax.Precision.HIGHEST


def prefix_2(part, axis, combine, identity):
    place = lax.axis_index(axis)
    gathered = jax.tree.map(lambda a: lax.all_gather(a, axis), part)
    state = jax.tree.map(lambda a, e: jnp.zeros_like(a) + jnp.asarray(e, a.dtype), part, identity)

    def one(hop, state):
        return combine(
            state, jax.tree.map(lambda a: lax.dynamic_index_in_dim(a, hop, 0, False), gathered)
        )

    return lax.fori_loop(0, place, one, state)


def unit_rows(array):
    floats = array.astype(jnp.float32)
    return floats * lax.rsqrt(jnp.sum(floats * floats, axis=-1, keepdims=True) + epsilon)


def to_blocks(array, count, length):
    return jnp.moveaxis(array.reshape((count, length) + array.shape[1:]), 2, 0)


def block_terms(query_blk, key_blk, value_blk, log_cum, strength):
    length = query_blk.shape[2]
    row_pos = lax.broadcasted_iota(jnp.int32, (length, length), 0)
    col_pos = lax.broadcasted_iota(jnp.int32, (length, length), 1)
    causal = row_pos >= col_pos
    spread = log_cum[..., :, None] - log_cum[..., None, :]
    decay = jnp.where(causal, jnp.exp(jnp.where(causal, spread, 0.0)), 0.0)
    key_key = jnp.einsum("hnid,hnjd->hnij", key_blk, key_blk, precision=exact_mode)
    lower = jnp.where(row_pos > col_pos, strength[..., :, None] * key_key * decay, 0.0)
    system = jnp.eye(length, dtype=jnp.float32) + lower
    right = jnp.concatenate(
        [value_blk * strength[..., None], key_blk * (strength * jnp.exp(log_cum))[..., None]],
        axis=-1,
    )
    solved = jax.scipy.linalg.solve_triangular(system, right, lower=True, unit_diagonal=True)
    width = value_blk.shape[-1]
    fixed_values = solved[..., :width]
    fixed_keys = solved[..., width:]
    query_key = jnp.einsum("hnid,hnjd->hnij", query_blk, key_blk, precision=exact_mode) * decay
    query_dec = query_blk * jnp.exp(log_cum)[..., None]
    key_dec = key_blk * jnp.exp(log_cum[..., -1:] - log_cum)[..., None]
    last_decay = jnp.exp(log_cum[..., -1])
    return (query_key, fixed_values, fixed_keys, query_dec, key_dec, last_decay)


def assemble_parameters(
    attention_queryset,
    attention_keyset,
    attention_valueset,
    retention_prelinear_score,
    additional_attenuation,
    feature_retention_logscale,
    strength_prelinear_score,
):
    tokens_here, heads = retention_prelinear_score.shape
    count = tokens_here // BLK
    query_all = unit_rows(attention_queryset.reshape(tokens_here, heads, HK)) * HK ** (-0.5)
    key_all = unit_rows(attention_keyset.reshape(tokens_here, heads, HK))
    value_all = attention_valueset.reshape(tokens_here, heads, HK).astype(jnp.float32)
    forgetting_exponent = (
        -jnp.exp(feature_retention_logscale)[None, :] * jax.nn.softplus(retention_prelinear_score)
        + additional_attenuation
    )
    log_cum = jnp.cumsum(to_blocks(forgetting_exponent, count, BLK), axis=-1)
    strength = jax.nn.sigmoid(to_blocks(strength_prelinear_score, count, BLK))
    return block_terms(
        to_blocks(query_all, count, BLK),
        to_blocks(key_all, count, BLK),
        to_blocks(value_all, count, BLK),
        log_cum,
        strength,
    )


def project(left, right):
    return jnp.einsum("hcd,hde->hce", left, right, precision=exact_mode)


def propagate(state, fresh, key_dec, last_decay):
    return state * last_decay[:, None, None] + jnp.einsum(
        "hcd,hce->hde", key_dec, fresh, precision=exact_mode
    )


def read_step(state, inputs):
    query_key, fixed_values, fixed_keys, query_dec, key_dec, last_decay = inputs
    fresh = fixed_values - project(fixed_keys, state)
    output = project(query_dec, state) + project(query_key, fresh)
    return (propagate(state, fresh, key_dec, last_decay), output)


def chain(earlier, later):
    first_map, first_shift = earlier
    second_map, second_shift = later
    return (project(second_map, first_map), project(second_map, first_shift) + second_shift)


def head_finish(outputs, readout_switch_preactivation, channel_rescale_vector):
    count, heads, length, width = outputs.shape
    flat = jnp.transpose(outputs, (0, 2, 1, 3)).reshape(count * length, heads, width)
    scaled = flat * lax.rsqrt(jnp.mean(flat * flat, axis=-1, keepdims=True) + epsilon)
    scaled = scaled * channel_rescale_vector.astype(jnp.float32)
    gate = readout_switch_preactivation.reshape(count * length, heads, width).astype(jnp.float32)
    return (scaled * jax.nn.silu(gate)).reshape(count * length, heads * width).astype(jnp.bfloat16)


def rms_gain(array, gain):
    floats = array.astype(jnp.float32)
    scaled = floats * lax.rsqrt(jnp.mean(floats * floats, axis=-1, keepdims=True) + epsilon)
    return (scaled * gain.astype(jnp.float32)).astype(jnp.bfloat16)


def expert_mlp(rows, gate_weight, up_weight, down_weight):
    gate = jnp.dot(rows, gate_weight, preferred_element_type=jnp.float32)
    upward = jnp.dot(rows, up_weight, preferred_element_type=jnp.float32)
    hidden = (jax.nn.silu(gate) * upward).astype(jnp.bfloat16)
    return jnp.dot(hidden, down_weight, preferred_element_type=jnp.float32).astype(jnp.bfloat16)


def local(
    attention_queryset,
    attention_keyset,
    attention_valueset,
    readout_switch_preactivation,
    retention_prelinear_score,
    additional_attenuation,
    feature_retention_logscale,
    strength_prelinear_score,
    channel_rescale_vector,
    final_projection_matrix,
    skip_stream,
    specialist_rescale_vector,
    specialist_switch_matrix,
    specialist_widen_matrix,
    specialist_contract_matrix,
    chosen_specialist_ids,
    dispatch_shares,
):
    portion_increments = assemble_parameters(
        attention_queryset,
        attention_keyset,
        attention_valueset,
        retention_prelinear_score,
        additional_attenuation,
        feature_retention_logscale,
        strength_prelinear_score,
    )
    piled_together = tuple(
        (jnp.moveaxis(element_entry, 1, 0) for element_entry in portion_increments)
    )
    heads = retention_prelinear_score.shape[1]
    identity_map = jnp.broadcast_to(jnp.eye(HK, dtype=jnp.float32), (heads, HK, HK))
    zero_state = jnp.zeros((heads, HK, HK), jnp.float32)

    def summarize(carry, inputs):
        transfer, offset = carry
        _, fixed_values, fixed_keys, _, key_dec, last_decay = inputs
        moved = propagate(transfer, -project(fixed_keys, transfer), key_dec, last_decay)
        shifted = propagate(offset, fixed_values - project(fixed_keys, offset), key_dec, last_decay)
        return ((moved, shifted), None)

    totals, _ = lax.scan(summarize, (identity_map, zero_state), piled_together)
    prefix = prefix_2(totals, "sp", chain, (identity_map, zero_state))
    start = prefix[1]
    _, outputs = lax.scan(read_step, start, piled_together)
    mixed = head_finish(outputs, readout_switch_preactivation, channel_rescale_vector)
    own_rows = lax.all_to_all(mixed, "tp", split_axis=0, concat_axis=1, tiled=True)
    merged = (
        skip_stream.astype(jnp.float32)
        + jnp.dot(own_rows, final_projection_matrix, preferred_element_type=jnp.float32)
    ).astype(jnp.bfloat16)
    normed = rms_gain(merged, specialist_rescale_vector)
    rows = normed.shape[0]
    width = normed.shape[1]
    topk = chosen_specialist_ids.shape[1]
    ranks_sp = lax.axis_size("sp")
    ranks_tp = lax.axis_size("tp")
    experts = ranks_sp * ranks_tp
    capacity = max(2, 2 * rows * topk // experts)
    flat_ids = chosen_specialist_ids.reshape(-1)
    member = (
        flat_ids[:, None] == lax.broadcasted_iota(jnp.int32, (rows * topk, experts), 1)
    ).astype(jnp.int32)
    ranking = jnp.sum(member * (jnp.cumsum(member, axis=0) - 1), axis=1)
    slot_index = flat_ids * capacity + ranking
    source_rows = jnp.repeat(normed, topk, axis=0)
    outgoing = jnp.zeros((experts * capacity, width), jnp.bfloat16).at[slot_index].set(source_rows)
    outgoing = outgoing.reshape(experts, capacity, width)
    arrived = lax.all_to_all(outgoing, ("sp", "tp"), split_axis=0, concat_axis=0, tiled=True)
    flat = arrived.reshape(-1, arrived.shape[-1])
    returned = lax.all_to_all(
        expert_mlp(
            flat,
            specialist_switch_matrix[0],
            specialist_widen_matrix[0],
            specialist_contract_matrix[0],
        ).reshape(arrived.shape),
        ("sp", "tp"),
        split_axis=0,
        concat_axis=0,
        tiled=True,
    )
    picked = returned.reshape(experts * capacity, width)[slot_index]
    picked = picked.astype(jnp.float32).reshape(rows, topk, width)
    summed = jnp.sum(picked * dispatch_shares[..., None], axis=1)
    return (merged.astype(jnp.float32) + summed).astype(jnp.bfloat16)


def solution(mesh):
    return jax.shard_map(
        local,
        mesh=mesh,
        in_specs=(
            P(("grp", "sp"), "tp"),
            P(("grp", "sp"), "tp"),
            P(("grp", "sp"), "tp"),
            P(("grp", "sp"), "tp"),
            P(("grp", "sp"), "tp"),
            P(("grp", "sp"), "tp"),
            P("tp"),
            P(("grp", "sp"), "tp"),
            P(),
            P(),
            P(("grp", "sp", "tp"), None),
            P(),
            P(("sp", "tp"), None, None),
            P(("sp", "tp"), None, None),
            P(("sp", "tp"), None, None),
            P(("grp", "sp", "tp"), None),
            P(("grp", "sp", "tp"), None),
        ),
        out_specs=P(("grp", "sp", "tp"), None),
        check_vma=False,
    )
```

profile of v0, /device:TPU:0, one launch (start us, length us, event | category | flops | bytes accessed | tf_op | source)
XLA Modules:
  0.0 256.4 jit_solution(17260022554708675781)
XLA Ops:
  3.8 1.8 reshape.197
  9.3 39.3 %custom-call.4 = f32[2,4,1,64,64]{3,4,2,1,0:T(8,128)S(1)} custom-call(f32[2,4,1,64,64]{4,3,2,1,0:T(8,128)S(1)} %fusion.52), custom_call_target="InvertDiagBlocksLowerTriangular" | custom-call | tf_op jit(solution)/shard_map/jit(_solve_triangular)/vmap(vmap())/triangular_solve | solution.py:50
  50.7 5.5 %while.39 = (s32[]{:T(128)}, f32[2,128,128]{2,1,0:T(8,128)S(1)}, f32[2,128,128]{2,1,0:T(8,128)S(1)}, f32[4,2]{1,0:T(4,128)S(1)}, f32[4,2,64,128]{3,2,1,0:T(8,128...) while((s32[]{:T(128)}, f32[2,128,128]{2,1,0:T(8,128)S(1)}, ...), condition=%wide.region_3.4_spmd.clone, body=%wide.region_2.3_spmd.clone.sunk | while | flops 100892672 | bytes 1378440 | solution.py:177
  56.2 9.1 %all-gather = f32[8,128,128]{2,1,0:T(8,128)} all-gather(f32[2,128,128]{2,1,0:T(8,128)S(1)} %get-tuple-element.134), channel_id=2, replica_groups=mesh['grp'=2,'sp'=4,'tp'=4] {'sp'}, dimensions={0}, use_global_device_ids=true | all-gather | bytes 655360 | tf_op jit(solution)/shard_map/all_gather | solution.py:16
  65.4 7.7 %all-gather.1 = f32[8,128,128]{2,1,0:T(8,128)} all-gather(f32[2,128,128]{2,1,0:T(8,128)S(1)} %get-tuple-element.135), channel_id=3, replica_groups=mesh['grp'=2,'sp'=4,'tp'=4] {'sp'}, dimensions={0}, use_global_device_ids=true | all-gather | bytes 655360 | tf_op jit(solution)/shard_map/all_gather | solution.py:16
  73.1 1.8 mul.230
  78.3 2.3 bitcast_multiply_fusion.1
  81.9 16.5 %while.38 = (s32[]{:T(128)}, f32[2,128,128]{2,1,0:T(8,128)S(1)}, f32[4,2,64,128]{3,2,1,0:T(8,128)}, f32[4,2]{1,0:T(4,128)}, f32[4,2,64,128]{3,2,1,0:T(8,128)S(1)...) while((s32[]{:T(128)}, f32[2,128,128]{2,1,0:T(8,128)S(1)}, ...), condition=%wide.region_8.9_spmd, body=%wide.region_7.8_spmd.sunk | while | flops 88178688 | bytes 1378945 | solution.py:180
  83.2 1.7 fusion.131
  87.3 1.7 fusion.131
  91.5 1.7 fusion.131
  102.0 4.9 %all-to-all-start = ((bf16[4,64,256]{2,1,0:T(8,128)(2,1)}), bf16[4,64,256]{2,1,0:T(8,128)(2,1)S(1)}, u32[]{:S(2)}, u32[]{:S(2)}) async-start(bf16[4,64,256]{2,1,0:T(8,128)(2,1)} %bitcast.30), calls=%async_computation | async-start | bytes 262144 | tf_op jit(solution)/shard_map/all_to_all | solution.py:182
  108.3 4.6 %all-to-all-done = bf16[4,64,256]{2,1,0:T(8,128)(2,1)S(1)} async-done(((bf16[4,64,256]{2,1,0:T(8,128)(2,1)}), bf16[4,64,256]{2,1,0:T(8,128)(2,1)S(1)}, u32[]{:S(2)}, u32[]{:S(2)}) %all-to-all-start) | async-done | bytes 131104 | tf_op jit(solution)/shard_map/all_to_all | solution.py:182
  113.0 3.2 %multiply_reduce_fusion.1 = (f32[64]{0:T(128)S(1)}, f32[64,2048]{1,0:T(8,128)S(1)}) fusion(bf16[64,1024]{1,0:T(8,128)(2,1)S(1)} %bitcast.218, bf16[1024,2048]{1,0:T(8,128)(2,1)} %param.32, bf16[64,2048]{1,0:T(8,128)(2,1)S(1)} %copy-done.2), kind=kOutput, calls=%fused_computation.77 | convolution fusion | flops 269221824 | bytes 5112064 | tf_op jit(solution)/shard_map/dot_general | solution.py:185
  117.8 2.1 reshape.212
  119.9 4.4 %scatter_custom_fusion = bf16[512,2048]{1,0:T(8,128)(2,1)} fusion(s32[256]{0:T(256)S(1)} %bitcast.224, bf16[256,2048]{1,0:T(8,128)(2,1)} %reshape.212, bf16[]{:T(256)} %constant.87.clone.1), kind=kCustom, calls=%fused_computation.68 | custom fusion | bytes 2097664 | tf_op jit(solution)/shard_map/scatter | solution.py:202
  124.4 56.4 %all_to_all.29 = bf16[16,32,2048]{2,1,0:T(8,128)(2,1)S(1)} all-to-all(bf16[16,32,2048]{2,1,0:T(8,128)(2,1)} %bitcast.204), channel_id=1, replica_groups=mesh['grp'=2,'sp'=4,'tp'=4] {'sp','tp'}, dimensions={0} | all-to-all | bytes 4194304 | tf_op jit(solution)/shard_map/all_to_all | solution.py:204
  182.1 2.2 fusion.38
  184.3 6.3 %convolution_convert_fusion = bf16[512,2048]{1,0:T(8,128)(2,1)} fusion(bf16[1,512,2048]{2,1,0:T(8,128)(2,1)S(1)} %copy-done, bf16[512,2048]{1,0:T(8,128)(2,1)} %bitcast.209, bf16[1,2048,512]{2,1,0:T(8,128)(2,1)} %param.36, f32[512,512]{1,0:T(8,128)} %fusion.38), kind=kOutput, calls=%fused_computation.47 | convolution fusion | flops 2150105088 | bytes 9437184 | tf_op jit(solution)/shard_map/dot_general | solution.py:132
  190.6 4.6 %all-to-all-start.2 = ((bf16[16,32,2048]{2,1,0:T(8,128)(2,1)}), bf16[16,32,2048]{2,1,0:T(8,128)(2,1)}, u32[]{:S(2)}, u32[]{:S(2)}) async-start(bf16[16,32,2048]{2,1,0:T(8,128)(2,1)} %bitcast.207), calls=%async_computation.2 | async-start | bytes 4194304 | tf_op jit(solution)/shard_map/all_to_all | solution.py:206
  195.3 49.2 %all-to-all-done.2 = bf16[16,32,2048]{2,1,0:T(8,128)(2,1)} async-done(((bf16[16,32,2048]{2,1,0:T(8,128)(2,1)}), bf16[16,32,2048]{2,1,0:T(8,128)(2,1)}, u32[]{:S(2)}, u32[]{:S(2)}) %all-to-all-start.2) | async-done | bytes 2097184 | tf_op jit(solution)/shard_map/all_to_all | solution.py:206
  244.5 5.2 %gather_fusion = bf16[256,2048]{1,0:T(8,128)(2,1)} fusion(bf16[512,2048]{1,0:T(8,128)(2,1)} %bitcast.41, s32[1024]{0:T(1024)S(1)} %pad_clamp_fusion), kind=kCustom, calls=%fused_computation | custom fusion | bytes 2098176 | tf_op jit(solution)/shard_map/gather | solution.py:218
  249.7 2.7 %reshape.198 = f32[64,4,2048]{2,1,0:T(4,128)} reshape(bf16[256,2048]{1,0:T(8,128)(2,1)} %gather_fusion) | data formatting | bytes 3145728 | tf_op jit(solution)/shard_map/convert_element_type | solution.py:219
  252.4 3.2 %multiply_reduce_fusion = f32[64,2048]{1,0:T(8,128)S(1)} fusion(f32[64,4,2048]{2,1,0:T(4,128)} %reshape.198, f32[64,4]{1,0:T(8,128)S(1)} %copy.132), kind=kLoop, calls=%fused_computation.56 | loop fusion | flops 917504 | bytes 2622464 | tf_op jit(solution)/shard_map/reduce_sum | solution.py:220
  (136 shorter events, 39.6 us)
Async XLA Ops:
  0.0 184.3 %copy-start = (bf16[1,512,2048]{2,1,0:T(8,128)(2,1)S(1)}, bf16[1,512,2048]{2,1,0:T(8,128)(2,1)}, u32[]{:S(2)}) copy-start(bf16[1,512,2048]{2,1,0:T(8,128)(2,1)} %param.37) | copy-start | bytes 6291460
  0.0 8.2 %copy-start.9 = (f32[256,2]{0,1:T(2,128)S(1)}, f32[256,2]{0,1:T(2,128)}, u32[]{:S(2)}) copy-start(f32[256,2]{0,1:T(2,128)} %param.30) | copy-start | bytes 6148
  0.0 48.6 %copy-start.3 = (bf16[256,256]{1,0:T(8,128)(2,1)S(1)}, bf16[256,256]{1,0:T(8,128)(2,1)}, u32[]{:S(2)}) copy-start(bf16[256,256]{1,0:T(8,128)(2,1)} %param.25) | copy-start | bytes 393220
  56.2 16.9 %copy-start.8 = (f32[4,2]{1,0:T(4,128)}, f32[4,2]{1,0:T(4,128)S(1)}, u32[]{:S(2)}) copy-start(f32[4,2]{1,0:T(4,128)S(1)} %get-tuple-element.513) | copy-start | bytes 100
  81.9 19.0 %copy-start.11 = (bf16[128]{0:T(256)(128)(2,1)S(1)}, bf16[128]{0:T(256)(128)(2,1)}, u32[]{:S(2)}) copy-start(bf16[128]{0:T(256)(128)(2,1)} %param.31) | copy-start | bytes 772
  81.9 19.3 %copy-start.4 = (bf16[256,256]{1,0:T(8,128)(2,1)S(1)}, bf16[256,256]{1,0:T(8,128)(2,1)}, u32[]{:S(2)}) copy-start(bf16[256,256]{1,0:T(8,128)(2,1)} %param.26) | copy-start | bytes 393220
  98.4 8.5 %copy-start.5 = (s32[64,4]{0,1:T(4,128)S(1)}, s32[64,4]{0,1:T(4,128)}, u32[]{:S(2)}) copy-start(s32[64,4]{0,1:T(4,128)} %param.38) | copy-start | bytes 3076
  98.4 8.8 %copy-start.6 = (bf16[2048]{0:T(1024)(128)(2,1)S(1)}, bf16[2048]{0:T(1024)(128)(2,1)}, u32[]{:S(2)}) copy-start(bf16[2048]{0:T(1024)(128)(2,1)} %param.34) | copy-start | bytes 12292
  98.4 14.6 %copy-start.2 = (bf16[64,2048]{1,0:T(8,128)(2,1)S(1)}, bf16[64,2048]{1,0:T(8,128)(2,1)}, u32[]{:S(2)}) copy-start(bf16[64,2048]{1,0:T(8,128)(2,1)} %param.33) | copy-start | bytes 786436
  102.0 11.0 %all-to-all-start = ((bf16[4,64,256]{2,1,0:T(8,128)(2,1)}), bf16[4,64,256]{2,1,0:T(8,128)(2,1)S(1)}, u32[]{:S(2)}, u32[]{:S(2)}) async-start(bf16[4,64,256]{2,1,0:T(8,128)(2,1)} %bitcast.30), calls=%async_computation | async-start | bytes 262144 | tf_op jit(solution)/shard_map/all_to_all | solution.py:182
  124.4 57.7 %copy-start.10 = (bf16[1,2048,512]{2,1,0:T(8,128)(2,1)S(1)}, bf16[1,2048,512]{2,1,0:T(8,128)(2,1)}, u32[]{:S(2)}) copy-start(bf16[1,2048,512]{2,1,0:T(8,128)(2,1)} %param.35) | copy-start | bytes 6291460
  180.8 1.3 copy-start.1
  190.6 4.6 %copy-start.7 = (f32[64,4]{0,1:T(4,128)S(1)}, f32[64,4]{0,1:T(4,128)}, u32[]{:S(2)}) copy-start(f32[64,4]{0,1:T(4,128)} %param.39) | copy-start | bytes 3076
  190.6 53.9 %all-to-all-start.2 = ((bf16[16,32,2048]{2,1,0:T(8,128)(2,1)}), bf16[16,32,2048]{2,1,0:T(8,128)(2,1)}, u32[]{:S(2)}, u32[]{:S(2)}) async-start(bf16[16,32,2048]{2,1,0:T(8,128)(2,1)} %bitcast.207), calls=%async_computation.2 | async-start | bytes 4194304 | tf_op jit(solution)/shard_map/all_to_all | solution.py:206
where the time goes:
time: 258 us; the launch traced here: 256 us
  blocking collectives  73.2 us (28%)
  other arithmetic  57.2 us (22%)
  waiting for transfers between devices  53.9 us (21%)
  local copies, waits for them, and re-layouts  32.2 us (12%)
  matrix products  29.7 us (12%)
  starting transfers between devices  9.44 us (4%)
    all_to_all x1, blocking collectives, local(): lax.all_to_all(outgoing, ('sp', 'tp'), split_axis=0, concat_axis=0, tiled...  56.4 us
    all_to_all x1, waiting for transfers between devices, local(): lax.all_to_all(expert_mlp(flat, specialist_switch_matrix[0], specialist_w...  49.2 us
    another operation x4, other arithmetic, block_terms(): jax.scipy.linalg.solve_triangular(system, right, lower=True, unit_diagona...  39.4 us
    all_gather x2, blocking collectives, prefix_2(): gathered = jax.tree.map(lambda a: lax.all_gather(a, axis), part)  16.8 us
    dot_general x20, matrix products, project(): return jnp.einsum('hcd,hde->hce', left, right, precision=exact_mode)  10.5 us
    dot_general x1, matrix products, expert_mlp(): jnp.dot(hidden, down_weight, preferred_element_type=jnp.float32)  6.27 us
    gather x1, local copies, waits for them, and re-layouts, local(): picked = returned.reshape(experts * capacity, width)[slot_index]  5.2 us
  transfers between devices with their start and end apart: 2, of which 2 were waited for; matrix products, arithmetic and copies ran while one was open for 1% of the time, Pallas kernels for 0%

commit v1 on v0

v1 whole, which is shorter than its diff:
```python
import functools

import jax
import jax.numpy as jnp
from jax import lax
from jax.experimental import pallas as pl
from jax.experimental.pallas import tpu as pltpu
from jax.sharding import PartitionSpec as P

HK = 128
epsilon = 1e-06
MESH = pl.DeviceIdType.MESH
VLIM = 64 * 1024 * 1024 - 128 * 1024


def split2(a):
    hi = a.astype(jnp.bfloat16)
    return hi, (a - hi.astype(jnp.float32)).astype(jnp.bfloat16)


def dims(ca, cb):
    return (((ca,), (cb,)), ((), ()))


def dot1(a, b, ca=1, cb=0):
    return lax.dot_general(a, b, dims(ca, cb), preferred_element_type=jnp.float32)


def dot3(a, b, ca=1, cb=0):
    return dot1(a[0], b[0], ca, cb) + (dot1(a[0], b[1], ca, cb) + dot1(a[1], b[0], ca, cb))


def attention_kernel(q_ref, k_ref, v_ref, ld_ref, st_ref, o_ref, qe_ref, m_ref, s_ref):
    length, heads = ld_ref.shape
    row = lax.broadcasted_iota(jnp.int32, (length, length), 0)
    col = lax.broadcasted_iota(jnp.int32, (length, length), 1)
    causal = row >= col
    strict = row > col
    tri = causal.astype(jnp.float32)
    ld = ld_ref[...]
    cum_col = lax.dot_general(tri, ld, dims(1, 0), precision=lax.Precision.HIGHEST,
                              preferred_element_type=jnp.float32)
    cum_row = lax.dot_general(ld, tri, dims(0, 1), precision=lax.Precision.HIGHEST,
                              preferred_element_type=jnp.float32)
    beta_all = jax.nn.sigmoid(st_ref[...])
    eye = (row == col).astype(jnp.float32)
    eye_k = (lax.broadcasted_iota(jnp.int32, (HK, HK), 0)
             == lax.broadcasted_iota(jnp.int32, (HK, HK), 1)).astype(jnp.float32)
    xs, lows, keep = [], [], []
    for h in range(heads):
        sl = slice(h * HK, (h + 1) * HK)
        q = q_ref[:, sl].astype(jnp.float32)
        k = k_ref[:, sl].astype(jnp.float32)
        v = v_ref[:, sl].astype(jnp.float32)
        q = q * lax.rsqrt(jnp.sum(q * q, axis=1, keepdims=True) + epsilon) * HK ** (-0.5)
        k = k * lax.rsqrt(jnp.sum(k * k, axis=1, keepdims=True) + epsilon)
        c = cum_col[:, h:h + 1]
        r = cum_row[h:h + 1, :]
        beta = beta_all[:, h:h + 1]
        decay = jnp.where(causal, jnp.exp(jnp.minimum(c - r, 0.0)), 0.0)
        ks = split2(k)
        lower = jnp.where(strict, beta * dot3(ks, ks, 1, 1) * decay, 0.0)
        scores = split2(dot3(split2(q), ks, 1, 1) * decay)
        lows.append(lower)
        keep.append((q, k, v, c, beta, scores))
        n = jnp.where((row // 8) == (col // 8), -lower, 0.0)
        n1 = split2(n)
        n2f = dot3(n1, n1)
        n2 = split2(n2f)
        p = eye + n
        p = p + dot3(split2(p), n2)
        n4 = split2(dot3(n2, n2))
        xs.append(p + dot3(split2(p), n4))
    size = 8
    while size < length:
        mask = ((row // (2 * size)) == (col // (2 * size))) & ((row // size) != (col // size))
        for h in range(heads):
            part = split2(jnp.where(mask, lows[h], 0.0))
            x2 = split2(xs[h])
            xs[h] = xs[h] - dot3(x2, split2(dot3(part, x2)))
        size *= 2
    for h in range(heads):
        sl = slice(h * HK, (h + 1) * HK)
        q, k, v, c, beta, scores = keep[h]
        up = jnp.exp(c)
        last = c[length - 1:length, :]
        right = jnp.concatenate([v * beta, k * (beta * up)], axis=1)
        uw = split2(dot3(split2(xs[h]), split2(right)))
        mixed = dot3(scores, uw)
        o_ref[:, sl] = mixed[:, :HK]
        qe_ref[:, sl] = q * up - mixed[:, HK:]
        ends = dot3(split2(k * jnp.exp(last - c)), uw, 0, 0)
        s_ref[h] = ends[:, :HK]
        m_ref[h] = jnp.exp(last) * eye_k - ends[:, HK:]


def attention_terms(q, k, v, log_decay, strength_pre):
    length, heads = log_decay.shape
    f32 = jnp.float32
    vm = pl.BlockSpec(memory_space=pltpu.VMEM)
    return pl.pallas_call(
        attention_kernel,
        out_shape=(
            jax.ShapeDtypeStruct((length, heads * HK), f32),
            jax.ShapeDtypeStruct((length, heads * HK), f32),
            jax.ShapeDtypeStruct((heads, HK, HK), f32),
            jax.ShapeDtypeStruct((heads, HK, HK), f32),
        ),
        in_specs=[vm] * 5,
        out_specs=(vm,) * 4,
        compiler_params=pltpu.CompilerParams(vmem_limit_bytes=32 * 1024 * 1024),
        name="attention_terms",
    )(q, k, v, log_decay, strength_pre)


def experts_kernel(ny, nz, rows, width, experts, x_ref, merged_ref, wg_hbm, wu_hbm, wd_hbm, out_ref,
                   G, Pt, CR, YR, ZR, wg, wu, wd, wsem, own_sem,
                   zs, zr, ys, yr, cs, cr, rcs, rcr, rys, ryr, rzs, rzr):
    sp = lax.axis_index("sp")
    z = lax.axis_index("tp")
    y = sp // 2
    c = sp % 2
    pc = 1 - c
    me = sp * nz + z
    expert = me
    f32 = jnp.float32

    def slot(yy, cc, zz):
        return (yy * 2 + cc) * nz + zz

    loads = [pltpu.make_async_copy(s, d, wsem.at[i])
             for i, (s, d) in enumerate(((wg_hbm, wg), (wu_hbm, wu), (wd_hbm, wd)))]
    for load in loads:
        load.start()
    own = pltpu.make_async_copy(x_ref, G.at[me], own_sem)
    own.start()

    barrier = pltpu.get_barrier_semaphore()
    greet = [{"tp": lax.rem(z + 1, nz)}, {"tp": lax.rem(z + nz - 1, nz)},
             {"sp": lax.rem(y + 1, ny) * 2 + c}, {"sp": lax.rem(y + ny - 1, ny) * 2 + c},
             {"sp": y * 2 + pc}]
    for d in greet:
        pl.semaphore_signal(barrier, inc=1, device_id=d, device_id_type=MESH)
    pl.semaphore_wait(barrier, len(greet))

    def remote(src, dst, ssem, rsem, dev):
        return pltpu.make_async_remote_copy(src_ref=src, dst_ref=dst, send_sem=ssem, recv_sem=rsem,
                                            device_id=dev, device_id_type=MESH)

    def z_copy(d, b, src=None):
        sl = slot(y, c, b)
        return remote(G.at[sl] if src is None else src, G.at[sl], zs.at[d, b], zr.at[b],
                      {"tp": z + (1 if d == 0 else -1)})

    def y_copy(d, yy, b, src=None):
        sl = slot(yy, c, b)
        return remote(G.at[sl] if src is None else src, G.at[sl], ys.at[d, yy, b], yr.at[yy, b],
                      {"sp": (y + (1 if d == 0 else -1)) * 2 + c})

    def c_copy(yy, b, cc=None, src=None):
        cc = c if cc is None else cc
        sl = slot(yy, cc, b)
        return remote(G.at[sl] if src is None else src, G.at[sl], cs.at[yy, b], cr.at[yy, b],
                      {"sp": y * 2 + pc})

    def fan_y(b, src=None):
        @pl.when(y + 1 < ny)
        def _():
            y_copy(0, y, b, src).start()

        @pl.when(y > 0)
        def _():
            y_copy(1, y, b, src).start()

    @pl.when(z + 1 < nz)
    def _():
        z_copy(0, z, x_ref).start()

    @pl.when(z > 0)
    def _():
        z_copy(1, z, x_ref).start()

    fan_y(z, x_ref)
    c_copy(y, z, src=x_ref).start()
    own.wait()

    @pl.loop(1, nz)
    def _(s):
        for d in (0, 1):
            b = z - s if d == 0 else z + s
            ok = b >= 0 if d == 0 else b < nz
            onward = z + 1 < nz if d == 0 else z > 0

            @pl.when(ok)
            def _():
                z_copy(d, b).wait_recv()

                @pl.when(onward)
                def _():
                    z_copy(d, b).start()

                fan_y(b)
                c_copy(y, b).start()

    def compute(yy, cc):
        first = slot(yy, cc, 0)
        x = jnp.concatenate([G[first + b, :, :width] for b in range(nz)], axis=0)
        tail = jnp.concatenate([G[first + b, :, width:] for b in range(nz)], axis=0).astype(f32)
        lane = lax.broadcasted_iota(jnp.int32, tail.shape, 1)
        share = jnp.sum(jnp.where((lane == expert) | (lane == expert + experts), tail, 0.0),
                        axis=1, keepdims=True)
        gate = jnp.dot(x, wg[...], preferred_element_type=f32)
        upward = jnp.dot(x, wu[...], preferred_element_type=f32)
        hidden = (jax.nn.silu(gate) * upward).astype(jnp.bfloat16)
        half = width // 2
        for i in range(2):
            cols = slice(i * half, (i + 1) * half)
            got = (jnp.dot(hidden, wd[:, cols], preferred_element_type=f32) * share).astype(jnp.bfloat16)
            for b in range(nz):
                Pt[first + b, :, cols] = got[b * rows:(b + 1) * rows]

    for load in loads:
        load.wait()

    @pl.loop(1, ny)
    def _(t):
        for d in (0, 1):
            yy = y - t if d == 0 else y + t
            ok = yy >= 0 if d == 0 else yy < ny
            onward = y + 1 < ny if d == 0 else y > 0

            @pl.when(ok)
            def _():
                @pl.loop(0, nz)
                def _(b):
                    y_copy(d, yy, b).wait_recv()

                    @pl.when(onward)
                    def _():
                        y_copy(d, yy, b).start()

                    c_copy(yy, b).start()

    def rc_copy(yy, b):
        return remote(Pt.at[slot(yy, pc, b)], CR.at[yy, b], rcs.at[yy, b], rcr.at[yy, b],
                      {"sp": y * 2 + pc})

    @pl.loop(0, 2 * ny)
    def _(j):
        yy = lax.rem(y + lax.rem(j, ny), ny)
        cc = jnp.where(j < ny, pc, c)

        @pl.when(j < ny)
        def _():
            @pl.loop(0, nz)
            def _(b):
                c_copy(yy, b, cc=pc).wait_recv()

        compute(yy, cc)

        @pl.when(j < ny)
        def _():
            @pl.loop(0, nz)
            def _(b):
                rc_copy(yy, b).start()

    def add_to(sl, other):
        Pt[sl] = (Pt[sl].astype(f32) + other.astype(f32)).astype(jnp.bfloat16)

    def ry_copy(d, yy, b):
        dest = y + (1 if d == 0 else -1)
        place = yy if d == 0 else jnp.where(yy == dest, ny, yy)
        return remote(Pt.at[slot(yy, c, b)], YR.at[place, b], rys.at[d, yy, b], ryr.at[place, b],
                      {"sp": dest * 2 + c})

    def ry_wait(place, b):
        remote(YR.at[place, b], YR.at[place, b], rys.at[0, 0, b], ryr.at[place, b],
               {"sp": y * 2 + pc}).wait_recv()

    @pl.loop(0, ny - 1)
    def _(t):
        for d in (0, 1):
            yy = ny - 1 - t if d == 0 else t
            ok = yy > y if d == 0 else yy < y
            behind = y > 0 if d == 0 else y + 1 < ny

            @pl.when(ok)
            def _():
                @pl.loop(0, nz)
                def _(i):
                    b = jnp.where(lax.rem(i, 2) == 0, nz - 1 - i // 2, i // 2)
                    sl = slot(yy, c, b)
                    rc_copy(yy, b).wait_recv()
                    add_to(sl, CR[yy, b])

                    @pl.when(behind)
                    def _():
                        ry_wait(yy, b)
                        add_to(sl, YR[yy, b])

                    ry_copy(d, yy, b).start()

    def rz_copy(d, b):
        dest = z + (1 if d == 0 else -1)
        place = b if d == 0 else jnp.where(b == dest, nz, b)
        return remote(Pt.at[slot(y, c, b)], ZR.at[place], rzs.at[d, b], rzr.at[place], {"tp": dest})

    def rz_wait(place):
        remote(ZR.at[place], ZR.at[place], rzs.at[0, 0], rzr.at[place], {"tp": z}).wait_recv()

    @pl.loop(0, nz)
    def _(i):
        b = jnp.where(lax.rem(i, 2) == 0, nz - 1 - i // 2, i // 2)
        sl = slot(y, c, b)
        rc_copy(y, b).wait_recv()
        add_to(sl, CR[y, b])

        @pl.when(y > 0)
        def _():
            ry_wait(y, b)
            add_to(sl, YR[y, b])

        @pl.when(y + 1 < ny)
        def _():
            ry_wait(ny, b)
            add_to(sl, YR[ny, b])

        for d in (0, 1):
            ok = b > z if d == 0 else b < z
            behind = z > 0 if d == 0 else z + 1 < nz

            @pl.when(ok)
            def _():
                @pl.when(behind)
                def _():
                    rz_wait(b)
                    add_to(sl, ZR[b])

                rz_copy(d, b).start()

    @pl.when(z > 0)
    def _():
        rz_wait(z)
        add_to(me, ZR[z])

    @pl.when(z + 1 < nz)
    def _():
        rz_wait(nz)
        add_to(me, ZR[nz])

    out_ref[...] = (merged_ref[...].astype(f32) + Pt[me].astype(f32)).astype(jnp.bfloat16)

    @pl.loop(0, nz)
    def _(b):
        @pl.when((z + 1 < nz) & (b <= z))
        def _():
            z_copy(0, b).wait_send()

        @pl.when((z > 0) & (b >= z))
        def _():
            z_copy(1, b).wait_send()

        @pl.when(b > z)
        def _():
            rz_copy(0, b).wait_send()

        @pl.when(b < z)
        def _():
            rz_copy(1, b).wait_send()

        @pl.loop(0, ny)
        def _(yy):
            c_copy(yy, b).wait_send()
            rc_copy(yy, b).wait_send()

            @pl.when((y + 1 < ny) & (yy <= y))
            def _():
                y_copy(0, yy, b).wait_send()

            @pl.when((y > 0) & (yy >= y))
            def _():
                y_copy(1, yy, b).wait_send()

            @pl.when(yy > y)
            def _():
                ry_copy(0, yy, b).wait_send()

            @pl.when(yy < y)
            def _():
                ry_copy(1, yy, b).wait_send()


def run_experts(payload, merged, wg, wu, wd, ny, nz, experts):
    rows, width = merged.shape
    wide = payload.shape[1]
    hidden = wg.shape[1]
    blocks = ny * 2 * nz
    bf = jnp.bfloat16
    vm = pl.BlockSpec(memory_space=pltpu.VMEM)
    hbm = pl.BlockSpec(memory_space=pl.ANY)
    dma = pltpu.SemaphoreType.DMA
    return pl.pallas_call(
        functools.partial(experts_kernel, ny, nz, rows, width, experts),
        out_shape=jax.ShapeDtypeStruct((rows, width), bf),
        in_specs=[vm, vm, hbm, hbm, hbm],
        out_specs=vm,
        scratch_shapes=[
            pltpu.VMEM((blocks, rows, wide), bf),
            pltpu.VMEM((blocks, rows, width), bf),
            pltpu.VMEM((ny, nz, rows, width), bf),
            pltpu.VMEM((ny + 1, nz, rows, width), bf),
            pltpu.VMEM((nz + 1, rows, width), bf),
            pltpu.VMEM((width, hidden), bf),
            pltpu.VMEM((width, hidden), bf),
            pltpu.VMEM((hidden, width), bf),
            dma((3,)), dma,
            dma((2, nz)), dma((nz,)),
            dma((2, ny, nz)), dma((ny, nz)),
            dma((ny, nz)), dma((ny, nz)),
            dma((ny, nz)), dma((ny, nz)),
            dma((2, ny, nz)), dma((ny + 1, nz)),
            dma((2, nz)), dma((nz + 1,)),
        ],
        compiler_params=pltpu.CompilerParams(
            collective_id=3, has_side_effects=True, vmem_limit_bytes=VLIM),
        name="routed_experts",
    )(payload, merged, wg, wu, wd)


def prefix_state(m, s, axis):
    place = lax.axis_index(axis)
    ms = lax.all_gather(jnp.concatenate([m, s], axis=-1), axis)

    def one(hop, state):
        got = lax.dynamic_index_in_dim(ms, hop, 0, False)
        return jnp.einsum("hcd,hde->hce", got[..., :HK], state, precision=lax.Precision.HIGHEST) + got[..., HK:]

    return lax.fori_loop(0, place, one, jnp.zeros_like(s))


def local(
    attention_queryset,
    attention_keyset,
    attention_valueset,
    readout_switch_preactivation,
    retention_prelinear_score,
    additional_attenuation,
    feature_retention_logscale,
    strength_prelinear_score,
    channel_rescale_vector,
    final_projection_matrix,
    skip_stream,
    specialist_rescale_vector,
    specialist_switch_matrix,
    specialist_widen_matrix,
    specialist_contract_matrix,
    chosen_specialist_ids,
    dispatch_shares,
):
    f32 = jnp.float32
    bf = jnp.bfloat16
    tokens, heads = retention_prelinear_score.shape
    nsp = lax.axis_size("sp")
    nz = lax.axis_size("tp")
    ny = nsp // 2
    experts = nsp * nz
    log_decay = (
        -jnp.exp(feature_retention_logscale)[None, :] * jax.nn.softplus(retention_prelinear_score)
        + additional_attenuation
    )
    o, qe, m, s = attention_terms(
        attention_queryset, attention_keyset, attention_valueset, log_decay, strength_prelinear_score)
    start = prefix_state(m, s, "sp")
    out = o.reshape(tokens, heads, HK) + jnp.einsum(
        "thd,hde->the", qe.reshape(tokens, heads, HK), start, precision=lax.Precision.HIGHEST)
    scaled = out * lax.rsqrt(jnp.mean(out * out, axis=-1, keepdims=True) + epsilon)
    scaled = scaled * channel_rescale_vector.astype(f32)
    gate = readout_switch_preactivation.reshape(tokens, heads, HK).astype(f32)
    mixed = (scaled * jax.nn.silu(gate)).reshape(tokens, heads * HK).astype(bf)
    own_rows = lax.all_to_all(mixed, "tp", split_axis=0, concat_axis=1, tiled=True)
    merged = (
        skip_stream.astype(f32)
        + jnp.dot(own_rows, final_projection_matrix, preferred_element_type=f32)
    ).astype(bf)
    floats = merged.astype(f32)
    normed = (floats * lax.rsqrt(jnp.mean(floats * floats, axis=-1, keepdims=True) + epsilon)
              * specialist_rescale_vector.astype(f32)).astype(bf)
    rows = normed.shape[0]
    lanes = -(-2 * experts // 128) * 128
    lane = lax.broadcasted_iota(jnp.int32, (rows, lanes), 1)
    tail = jnp.zeros((rows, lanes), f32)
    for i in range(chosen_specialist_ids.shape[1]):
        share = dispatch_shares[:, i:i + 1]
        high = share.astype(bf).astype(f32)
        chosen = chosen_specialist_ids[:, i:i + 1]
        tail = tail + jnp.where(lane == chosen, high, 0.0)
        tail = tail + jnp.where(lane == chosen + experts, share - high, 0.0)
    payload = jnp.concatenate([normed, tail.astype(bf)], axis=1)
    return run_experts(payload, merged, specialist_switch_matrix[0], specialist_widen_matrix[0],
                       specialist_contract_matrix[0], ny, nz, experts)


def solution(mesh):
    return jax.shard_map(
        local,
        mesh=mesh,
        in_specs=(
            P(("grp", "sp"), "tp"),
            P(("grp", "sp"), "tp"),
            P(("grp", "sp"), "tp"),
            P(("grp", "sp"), "tp"),
            P(("grp", "sp"), "tp"),
            P(("grp", "sp"), "tp"),
            P("tp"),
            P(("grp", "sp"), "tp"),
            P(),
            P(),
            P(("grp", "sp", "tp"), None),
            P(),
            P(("sp", "tp"), None, None),
            P(("sp", "tp"), None, None),
            P(("sp", "tp"), None, None),
            P(("grp", "sp", "tp"), None),
            P(("grp", "sp", "tp"), None),
        ),
        out_specs=P(("grp", "sp", "tp"), None),
        check_vma=False,
    )
```

time: 258 us -> 147 us (0.57)
  the two profiles are of different devices: /device:TPU:0 before, /device:TPU:10 now
where the time goes in v1:
time: 147 us; the launch traced here: 146 us
  Pallas kernels  88.2 us (60%)
  waiting for transfers between devices  18.7 us (13%)
  between operations  13.6 us (9%)
  local copies, waits for them, and re-layouts  9.7 us (7%)
  other arithmetic  7.28 us (5%)
  starting transfers between devices  5.14 us (3%)
  matrix products  3.6 us (2%)
    pallas_call x1, Pallas kernels, run_experts(): pl.pallas_call(functools.partial(experts_kernel, ny, nz, rows, width, exp...  81.4 us
    all_gather x1, waiting for transfers between devices, prefix_state(): ms = lax.all_gather(jnp.concatenate([m, s], axis=-1), axis)  13 us
    unnamed x14, local copies, waits for them, and re-layouts  7.5 us
    pallas_call x1, Pallas kernels, attention_terms(): pl.pallas_call(attention_kernel, out_shape=(jax.ShapeDtypeStruct((length,...  6.83 us
    all_to_all x1, waiting for transfers between devices, local(): lax.all_to_all(mixed, 'tp', split_axis=0, concat_axis=1, tiled=True)  5.7 us
    all_to_all x1, starting transfers between devices, local(): lax.all_to_all(mixed, 'tp', split_axis=0, concat_axis=1, tiled=True)  5.14 us
    dot_general x1, matrix products, local(): jnp.dot(own_rows, final_projection_matrix, preferred_element_type=f32)  3.17 us
  transfers between devices with their start and end apart: 2, of which 2 were waited for; matrix products, arithmetic and copies ran while one was open for 4% of the time, Pallas kernels for 0%

profile of v1, /device:TPU:10, one launch (start us, length us, event | category | flops | bytes accessed | tf_op | source)
XLA Modules:
  0.0 146.2 jit_solution(5906191193850227318)
XLA Ops:
  6.5 0.8 copy.56
  7.4 0.8 ne.4
  8.1 0.8 copy.58
  9.1 0.7 exponential_negate_fusion
  9.8 0.8 copy.59.st_ref
  10.7 0.9 copy-done
  11.6 0.9 copy-done.1
  12.5 0.9 copy-done.2
  13.4 6.8 %attention_terms.1 = (f32[256,256]{1,0:T(8,128)S(1)}, f32[256,256]{1,0:T(8,128)S(1)}, f32[2,128,128]{2,1,0:T(8,128)S(1)}, f32[2,128,128]{2,1,0:T(8,128)S(1)}) custom-call(bf16[256,256]{1,0:T(8,128)(2,1)S(1)} %copy-done, bf16[256,256]{1,0:T(8,128)(2,1)S(1)} %copy-done.1, bf16[256,256]{1,0:T(8,128)(2,1)S(1)} %copy-done.2, ...), custom_call_target="tpu_custom_call" | custom-call | tf_op jit(solution)/shard_map/attention_terms/pallas_call | solution.py:101
  20.3 0.7 pad_maximum_fusion.1
  21.1 1.0 copy.63
  22.8 0.7 convert_element_type.66
  23.5 0.8 convert_bitcast_fusion.3
  24.3 0.8 subtract_bitcast_fusion.3
  25.2 0.8 slice_bitcast_fusion.3
  26.0 13.0 %all-gather.3.cloned.1.call-done = f32[8,128,256]{2,1,0:T(8,128)} async-done(((f32[2,128,256]{2,1,0:T(8,128)}), f32[8,128,256]{2,1,0:T(8,128)}) %all-gather.3.cloned.1.call-update) | async-done | bytes 1048592 | tf_op jit(solution)/shard_map/all_gather | solution.py:432
  39.7 0.7 convert_element_type.63
  40.5 5.1 %all-to-all-start = ((bf16[4,64,256]{2,1,0:T(8,128)(2,1)}), bf16[4,64,256]{2,1,0:T(8,128)(2,1)S(1)}, u32[]{:S(2)}, u32[]{:S(2)}) async-start(bf16[4,64,256]{2,1,0:T(8,128)(2,1)} %convert_element_type.63), calls=%async_computation | async-start | bytes 262144 | tf_op jit(solution)/shard_map/all_to_all | solution.py:480
  45.8 5.7 %all-to-all-done = bf16[4,64,256]{2,1,0:T(8,128)(2,1)S(1)} async-done(((bf16[4,64,256]{2,1,0:T(8,128)(2,1)}), bf16[4,64,256]{2,1,0:T(8,128)(2,1)S(1)}, u32[]{:S(2)}, u32[]{:S(2)}) %all-to-all-start) | async-done | bytes 131104 | tf_op jit(solution)/shard_map/all_to_all | solution.py:480
  51.5 3.2 %fusion.3 = (f32[64]{0:T(128)S(1)}, bf16[64,2048]{1,0:T(8,128)(2,1)S(1)}) fusion(bf16[64,1024]{1,0:T(8,128)(2,1)S(1)} %bitcast.70, bf16[1024,2048]{1,0:T(8,128)(2,1)} %param.28, bf16[64,2048]{1,0:T(8,128)(2,1)S(1)} %copy-done.4), kind=kOutput, calls=%fused_computation.9 | convolution fusion | flops 269221824 | bytes 4849920 | tf_op jit(solution)/shard_map/dot_general | solution.py:483
  54.7 0.7 copy-done.3
  55.6 0.7 pad_maximum_fusion.x_ref
  56.3 81.4 %routed_experts.1 = bf16[64,2048]{1,0:T(8,128)(2,1)} custom-call(bf16[64,2176]{1,0:T(8,128)(2,1)} %pad_maximum_fusion.x_ref, bf16[64,2048]{1,0:T(8,128)(2,1)} %copy-done.3, bf16[2048,512]{1,0:T(8,128)(2,1)} %bitcast.64, bf16[2048,512]{1,0:T(8,128)(2,1)} %bitcast.65, bf16[512,2048]{1,0:T(8,128)(2,1)} %bitcast.66), custom_call_target="tpu_custom_call" | custom-call | tf_op jit(solution)/shard_map/routed_experts/pallas_call | solution.py:402
  137.7 1.7 %copy.87 = bf16[64,2048]{1,0:T(8,128)(2,1)} copy(bf16[64,2048]{1,0:T(8,128)(2,1)} %routed_experts.1) | data formatting | bytes 524288
  (22 shorter events, 2.1 us)
Async XLA Ops:
  6.5 32.5 %all-gather.3.cloned.1.call-start = ((), (), s32[]{:S(2)}) async-start(), calls=%async_computation.1 | async-start | bytes 1310720 | tf_op jit(solution)/shard_map/all_gather | solution.py:432
  10.7 0.9 copy-start
  11.6 0.9 copy-start.1
  12.5 0.9 copy-start.2
  39.0 12.5 %copy-start.4 = (bf16[64,2048]{1,0:T(8,128)(2,1)S(1)}, bf16[64,2048]{1,0:T(8,128)(2,1)}, u32[]{:S(2)}) copy-start(bf16[64,2048]{1,0:T(8,128)(2,1)} %param.29) | copy-start | bytes 786436
  40.5 11.0 %all-to-all-start = ((bf16[4,64,256]{2,1,0:T(8,128)(2,1)}), bf16[4,64,256]{2,1,0:T(8,128)(2,1)S(1)}, u32[]{:S(2)}, u32[]{:S(2)}) async-start(bf16[4,64,256]{2,1,0:T(8,128)(2,1)} %convert_element_type.63), calls=%async_computation | async-start | bytes 262144 | tf_op jit(solution)/shard_map/all_to_all | solution.py:480
  54.7 0.7 copy-start.3
Sparse Core Ops, SparseCore 0:
  21.1 17.8 all-gather.2

commit v2 on v1

--- a/solution.py
+++ b/solution.py
@@ -30,20 +30,39 @@
     return dot1(a[0], b[0], ca, cb) + (dot1(a[0], b[1], ca, cb) + dot1(a[1], b[0], ca, cb))
 
 
-def attention_kernel(q_ref, k_ref, v_ref, ld_ref, st_ref, o_ref, qe_ref, m_ref, s_ref):
-    length, heads = ld_ref.shape
+def attention_kernel(q_ref, k_ref, v_ref, g_ref, sc_ref, ad_ref, ls_ref, st_ref, gain_ref, wo_hbm, skip_ref,
+                     rescale_ref, ids_ref, share_ref, pay_ref, merged_ref,
+                     o_ref, qe_ref, m_ref, s_ref, start_ref, next_ref, mixed_ref, own_ref, wo,
+                     wsem, chain_s, chain_r, swap_s, swap_r):
+    heads, length = sc_ref.shape
+    f32 = jnp.float32
+    sp = lax.axis_index("sp")
+    z = lax.axis_index("tp")
+    nsp = lax.axis_size("sp")
+    nz = lax.axis_size("tp")
+    rows, width = merged_ref.shape
+    load = pltpu.make_async_copy(wo_hbm, wo, wsem)
+    load.start()
+    barrier = pltpu.get_barrier_semaphore()
+    greet = [{"sp": lax.rem(sp + 1, nsp)}, {"sp": lax.rem(sp + nsp - 1, nsp)}]
+    greet += [{"tp": lax.rem(z + d, nz)} for d in range(1, nz)]
+    for d in greet:
+        pl.semaphore_signal(barrier, inc=1, device_id=d, device_id_type=MESH)
     row = lax.broadcasted_iota(jnp.int32, (length, length), 0)
     col = lax.broadcasted_iota(jnp.int32, (length, length), 1)
     causal = row >= col
     strict = row > col
     tri = causal.astype(jnp.float32)
-    ld = ld_ref[...]
-    cum_col = lax.dot_general(tri, ld, dims(1, 0), precision=lax.Precision.HIGHEST,
+    score = sc_ref[...]
+    soft = jnp.maximum(score, 0.0) + jnp.log1p(jnp.exp(-jnp.abs(score)))
+    ld = ad_ref[...] - jnp.exp(ls_ref[...]) * soft
+    cum_col = lax.dot_general(tri, ld, dims(1, 1), precision=lax.Precision.HIGHEST,
                               preferred_element_type=jnp.float32)
-    cum_row = lax.dot_general(ld, tri, dims(0, 1), precision=lax.Precision.HIGHEST,
+    cum_row = lax.dot_general(ld, tri, dims(1, 1), precision=lax.Precision.HIGHEST,
                               preferred_element_type=jnp.float32)
-    beta_all = jax.nn.sigmoid(st_ref[...])
     eye = (row == col).astype(jnp.float32)
+    beta_all = lax.dot_general(eye, jax.nn.sigmoid(st_ref[...]), dims(1, 1), precision=lax.Precision.HIGHEST,
+                               preferred_element_type=jnp.float32)
     eye_k = (lax.broadcasted_iota(jnp.int32, (HK, HK), 0)
              == lax.broadcasted_iota(jnp.int32, (HK, HK), 1)).astype(jnp.float32)
     xs, lows, keep = [], [], []
@@ -93,24 +112,113 @@
         s_ref[h] = ends[:, :HK]
         m_ref[h] = jnp.exp(last) * eye_k - ends[:, HK:]
 
-
-def attention_terms(q, k, v, log_decay, strength_pre):
-    length, heads = log_decay.shape
-    f32 = jnp.float32
+    pl.semaphore_wait(barrier, len(greet))
+
+    def pass_on(to):
+        return pltpu.make_async_remote_copy(src_ref=next_ref, dst_ref=start_ref, send_sem=chain_s,
+                                            recv_sem=chain_r, device_id={"sp": to}, device_id_type=MESH)
+
+    @pl.when(sp == 0)
+    def _():
+        next_ref[...] = s_ref[...]
+        pass_on(1).start()
+
+    @pl.when(sp > 0)
+    def _():
+        pass_on(0).wait_recv()
+
+        @pl.when(sp < nsp - 1)
+        def _():
+            for h in range(heads):
+                next_ref[h] = s_ref[h] + dot3(split2(m_ref[h]), split2(start_ref[h]))
+            pass_on(sp + 1).start()
+
+        for h in range(heads):
+            sl = slice(h * HK, (h + 1) * HK)
+            o_ref[:, sl] += dot3(split2(qe_ref[:, sl]), split2(start_ref[h]))
+
+    gain = gain_ref[...].astype(f32)
+    for h in range(heads):
+        sl = slice(h * HK, (h + 1) * HK)
+        out = o_ref[:, sl]
+        out = out * lax.rsqrt(jnp.mean(out * out, axis=1, keepdims=True) + epsilon) * gain
+        mixed_ref[:, sl] = (out * jax.nn.silu(g_ref[:, sl].astype(f32))).astype(jnp.bfloat16)
+
+    def swap(d):
+        to = lax.rem(z + d, nz)
+        return pltpu.make_async_remote_copy(
+            src_ref=mixed_ref.at[pl.ds(to * rows, rows)], dst_ref=own_ref.at[z], send_sem=swap_s.at[d],
+            recv_sem=swap_r.at[d], device_id={"tp": to}, device_id_type=MESH)
+
+    for d in range(1, nz):
+        swap(d).start()
+    own_ref[z] = mixed_ref[pl.ds(z * rows, rows), :]
+    experts = nsp * nz
+    lanes = pay_ref.shape[1] - width
+    place = lax.broadcasted_iota(jnp.int32, (lanes, rows), 0)
+    table = jnp.zeros((lanes, rows), f32)
+    for i in range(ids_ref.shape[0]):
+        share = share_ref[i:i + 1, :]
+        high = share.astype(jnp.bfloat16).astype(f32)
+        chosen = ids_ref[i:i + 1, :]
+        table = table + jnp.where(place == chosen, high, 0.0)
+        table = table + jnp.where(place == chosen + experts, share - high, 0.0)
+    eye_r = (lax.broadcasted_iota(jnp.int32, (rows, rows), 0)
+             == lax.broadcasted_iota(jnp.int32, (rows, rows), 1)).astype(jnp.bfloat16)
+    pay_ref[:, width:] = dot1(eye_r, table.astype(jnp.bfloat16), 1, 1).astype(jnp.bfloat16)
+    load.wait()
+    for d in range(1, nz):
+        swap(d).wait_recv()
+    flat = jnp.concatenate([own_ref[t] for t in range(nz)], axis=1)
+    step = width // 4
+    total = jnp.zeros((rows, 1), f32)
+    for i in range(4):
+        cols = slice(i * step, (i + 1) * step)
+        got = (skip_ref[:, cols].astype(f32) + dot1(flat, wo[:, cols])).astype(jnp.bfloat16)
+        merged_ref[:, cols] = got
+        got = got.astype(f32)
+        total = total + jnp.sum(got * got, axis=1, keepdims=True)
+    scale = lax.rsqrt(total * (1.0 / width) + epsilon)
+    for i in range(4):
+        cols = slice(i * step, (i + 1) * step)
+        pay_ref[:, cols] = (merged_ref[:, cols].astype(f32) * scale
+                            * rescale_ref[:, cols].astype(f32)).astype(jnp.bfloat16)
+
+    @pl.when(sp < nsp - 1)
+    def _():
+        pass_on(sp + 1).wait_send()
+
+    for d in range(1, nz):
+        swap(d).wait_send()
+
+
+def attend(q, k, v, gate, score, added, logscale, strength_pre, gain, wo, skip, rescale, ids, shares, nz, lanes):
+    heads, length = score.shape
+    rows, width = skip.shape
+    f32, bf = jnp.float32, jnp.bfloat16
     vm = pl.BlockSpec(memory_space=pltpu.VMEM)
+    dma = pltpu.SemaphoreType.DMA
     return pl.pallas_call(
         attention_kernel,
-        out_shape=(
-            jax.ShapeDtypeStruct((length, heads * HK), f32),
-            jax.ShapeDtypeStruct((length, heads * HK), f32),
-            jax.ShapeDtypeStruct((heads, HK, HK), f32),
-            jax.ShapeDtypeStruct((heads, HK, HK), f32),
-        ),
-        in_specs=[vm] * 5,
-        out_specs=(vm,) * 4,
-        compiler_params=pltpu.CompilerParams(vmem_limit_bytes=32 * 1024 * 1024),
-        name="attention_terms",
-    )(q, k, v, log_decay, strength_pre)
+        out_shape=(jax.ShapeDtypeStruct((rows, width + lanes), bf), jax.ShapeDtypeStruct((rows, width), bf)),
+        in_specs=[vm] * 9 + [pl.BlockSpec(memory_space=pl.ANY)] + [vm] * 4,
+        out_specs=(vm, vm),
+        scratch_shapes=[
+            pltpu.VMEM((length, heads * HK), f32),
+            pltpu.VMEM((length, heads * HK), f32),
+            pltpu.VMEM((heads, HK, HK), f32),
+            pltpu.VMEM((heads, HK, HK), f32),
+            pltpu.VMEM((heads, HK, HK), f32),
+            pltpu.VMEM((heads, HK, HK), f32),
+            pltpu.VMEM((length, heads * HK), bf),
+            pltpu.VMEM((nz, rows, heads * HK), bf),
+            pltpu.VMEM(wo.shape, bf),
+            dma, dma, dma, dma((nz,)), dma((nz,)),
+        ],
+        compiler_params=pltpu.CompilerParams(
+            collective_id=5, has_side_effects=True, vmem_limit_bytes=48 * 1024 * 1024),
+        name="attend",
+    )(q, k, v, gate, score, added, logscale, strength_pre, gain, wo, skip, rescale, ids, shares)
 
 
 def experts_kernel(ny, nz, rows, width, experts, x_ref, merged_ref, wg_hbm, wu_hbm, wd_hbm, out_ref,
@@ -427,17 +535,6 @@
     )(payload, merged, wg, wu, wd)
 
 
-def prefix_state(m, s, axis):
-    place = lax.axis_index(axis)
-    ms = lax.all_gather(jnp.concatenate([m, s], axis=-1), axis)
-
-    def one(hop, state):
-        got = lax.dynamic_index_in_dim(ms, hop, 0, False)
-        return jnp.einsum("hcd,hde->hce", got[..., :HK], state, precision=lax.Precision.HIGHEST) + got[..., HK:]
-
-    return lax.fori_loop(0, place, one, jnp.zeros_like(s))
-
-
 def local(
     attention_queryset,
     attention_keyset,
@@ -457,47 +554,30 @@
     chosen_specialist_ids,
     dispatch_shares,
 ):
-    f32 = jnp.float32
-    bf = jnp.bfloat16
-    tokens, heads = retention_prelinear_score.shape
     nsp = lax.axis_size("sp")
     nz = lax.axis_size("tp")
-    ny = nsp // 2
     experts = nsp * nz
-    log_decay = (
-        -jnp.exp(feature_retention_logscale)[None, :] * jax.nn.softplus(retention_prelinear_score)
-        + additional_attenuation
+    lanes = -(-2 * experts // 128) * 128
+    payload, merged = attend(
+        attention_queryset,
+        attention_keyset,
+        attention_valueset,
+        readout_switch_preactivation,
+        retention_prelinear_score.T,
+        additional_attenuation.T,
+        feature_retention_logscale[:, None],
+        strength_prelinear_score.T,
+        channel_rescale_vector[None, :],
+        final_projection_matrix,
+        skip_stream,
+        specialist_rescale_vector[None, :],
+        chosen_specialist_ids.T,
+        dispatch_shares.T,
+        nz,
+        lanes,
     )
-    o, qe, m, s = attention_terms(
-        attention_queryset, attention_keyset, attention_valueset, log_decay, strength_prelinear_score)
-    start = prefix_state(m, s, "sp")
-    out = o.reshape(tokens, heads, HK) + jnp.einsum(
-        "thd,hde->the", qe.reshape(tokens, heads, HK), start, precision=lax.Precision.HIGHEST)
-    scaled = out * lax.rsqrt(jnp.mean(out * out, axis=-1, keepdims=True) + epsilon)
-    scaled = scaled * channel_rescale_vector.astype(f32)
-    gate = readout_switch_preactivation.reshape(tokens, heads, HK).astype(f32)
-    mixed = (scaled * jax.nn.silu(gate)).reshape(tokens, heads * HK).astype(bf)
-    own_rows = lax.all_to_all(mixed, "tp", split_axis=0, concat_axis=1, tiled=True)
-    merged = (
-        skip_stream.astype(f32)
-        + jnp.dot(own_rows, final_projection_matrix, preferred_element_type=f32)
-    ).astype(bf)
-    floats = merged.astype(f32)
-    normed = (floats * lax.rsqrt(jnp.mean(floats * floats, axis=-1, keepdims=True) + epsilon)
-              * specialist_rescale_vector.astype(f32)).astype(bf)
-    rows = normed.shape[0]
-    lanes = -(-2 * experts // 128) * 128
-    lane = lax.broadcasted_iota(jnp.int32, (rows, lanes), 1)
-    tail = jnp.zeros((rows, lanes), f32)
-    for i in range(chosen_specialist_ids.shape[1]):
-        share = dispatch_shares[:, i:i + 1]
-        high = share.astype(bf).astype(f32)
-        chosen = chosen_specialist_ids[:, i:i + 1]
-        tail = tail + jnp.where(lane == chosen, high, 0.0)
-        tail = tail + jnp.where(lane == chosen + experts, share - high, 0.0)
-    payload = jnp.concatenate([normed, tail.astype(bf)], axis=1)
     return run_experts(payload, merged, specialist_switch_matrix[0], specialist_widen_matrix[0],
-                       specialist_contract_matrix[0], ny, nz, experts)
+                       specialist_contract_matrix[0], nsp // 2, nz, experts)
 
 
 def solution(mesh):

time: 147 us -> 116 us (0.79)
  waiting for transfers between devices: 18.7 us -> 0 us
  between operations: 13.6 us -> 0.04 us
  Pallas kernels: 88.2 us -> 101 us
  other arithmetic: 7.28 us -> 0 us
  local copies, waits for them, and re-layouts: 9.7 us -> 15.3 us
  starting transfers between devices: 5.14 us -> 0 us
  matrix products: 3.6 us -> 0 us
    all_gather x1 -> x0, waiting for transfers between devices: 13 us -> none  [prefix_state(): ms = lax.all_gather(jnp.concatenate([m, s], axis=-1), axis)]
    pallas_call x1, Pallas kernels: 6.83 us -> 13.6 us  [attend(): pl.pallas_call(attention_kernel, out_shape=(jax.ShapeDtypeStruct((rows, w...]
    unnamed x14 -> x29, local copies, waits for them, and re-layouts: 7.5 us -> 13.9 us
    all_to_all x1 -> x0, waiting for transfers between devices: 5.7 us -> none  [local(): lax.all_to_all(mixed, 'tp', split_axis=0, concat_axis=1, tiled=True)]
    pallas_call x1, Pallas kernels: 81.4 us -> 87 us  [run_experts(): pl.pallas_call(functools.partial(experts_kernel, ny, nz, rows, width, exp...]
    all_to_all x1 -> x0, starting transfers between devices: 5.14 us -> none  [local(): lax.all_to_all(mixed, 'tp', split_axis=0, concat_axis=1, tiled=True)]
    dot_general x2 -> x0, matrix products: 3.6 us -> none  [the longest x1 3.17 us: local(): jnp.dot(own_rows, final_projection_matrix, preferred_element_type=f32)]
    convert_element_type x3 -> x0, local copies, waits for them, and re-layouts: 1.87 us -> none  [the longest x1 1 us: local(): gate = readout_switch_preactivation.reshape(tokens, heads, HK).astype(f32)]
  transfers between devices with their start and end apart: 2 -> 0, of which waited for: 2 -> 0; matrix products, arithmetic and copies ran while one was open for 4% -> 0% of each run, Pallas kernels for 0% -> 0%
where the time goes in v2:
time: 116 us
  Pallas kernels  101 us (87%)
  local copies, waits for them, and re-layouts  15.3 us (13%)
    pallas_call x1, Pallas kernels, run_experts(): pl.pallas_call(functools.partial(experts_kernel, ny, nz, rows, width, exp...  87 us
    unnamed x29, local copies, waits for them, and re-layouts  13.9 us
    pallas_call x1, Pallas kernels, attend(): pl.pallas_call(attention_kernel, out_shape=(jax.ShapeDtypeStruct((rows, w...  13.6 us

profile of v2, /device:TPU:10, one launch (start us, length us, event | category | flops | bytes accessed | tf_op | source)
XLA Modules:
  0.0 115.9 jit_solution(11600099551691523462)
XLA Ops:
  0.0 0.7 copy.18.ls_ref
  0.7 0.7 broadcast_in_dim.11.rescale_ref
  1.4 0.0 copy-start
  1.4 2.2 %copy-done = bf16[1024,2048]{1,0:T(8,128)(2,1)S(1)} copy-done((bf16[1024,2048]{1,0:T(8,128)(2,1)S(1)}, bf16[1024,2048]{1,0:T(8,128)(2,1)}, u32[]{:S(2)}) %copy-start) | copy-done | bytes 4194328
  3.6 0.0 copy-start.3
  3.6 0.9 copy-done.3
  4.6 0.0 copy-start.4
  4.6 0.9 copy-done.4
  5.5 0.0 copy-start.5
  5.5 0.9 copy-done.5
  6.4 0.9 copy-done.6
  7.3 0.9 copy-done.7
  8.2 0.7 copy-done.8
  8.9 0.7 copy-done.9
  9.6 0.7 copy-done.10
  10.2 0.7 copy-done.11
  10.9 0.7 copy-done.12
  11.6 0.7 copy-done.13
  12.3 13.6 %attend.1 = (bf16[64,2176]{1,0:T(8,128)(2,1)S(1)}, bf16[64,2048]{1,0:T(8,128)(2,1)S(1)}) custom-call(bf16[256,256]{1,0:T(8,128)(2,1)S(1)} %copy-done.4, bf16[256,256]{1,0:T(8,128)(2,1)S(1)} %copy-done.5, bf16[256,256]{1,0:T(8,128)(2,1)S(1)} %copy-done.6, bf16[256,256]{1,0:T(8,128)(2,1)S(1)} %copy-done.7, f32[2,256]{1,0:T(2,128)S(1)} %bitcast.10, ...), custom_call_target="tpu_custom_call" | custom-call | tf_op jit(solution)/shard_map/attend/pallas_call | solution.py:201
  25.9 0.0 copy-start.1
  25.9 0.7 copy-done.1
  26.6 0.7 copy-done.2
  27.3 87.0 %routed_experts.1 = bf16[64,2048]{1,0:T(8,128)(2,1)} custom-call(bf16[64,2176]{1,0:T(8,128)(2,1)} %copy-done.1, bf16[64,2048]{1,0:T(8,128)(2,1)} %copy-done.2, bf16[2048,512]{1,0:T(8,128)(2,1)} %bitcast.16, bf16[2048,512]{1,0:T(8,128)(2,1)} %bitcast.17, bf16[512,2048]{1,0:T(8,128)(2,1)} %bitcast.18), custom_call_target="tpu_custom_call" | custom-call | tf_op jit(solution)/shard_map/routed_experts/pallas_call | solution.py:510
  114.3 1.7 %copy.20 = bf16[64,2048]{1,0:T(8,128)(2,1)} copy(bf16[64,2048]{1,0:T(8,128)(2,1)} %routed_experts.1) | data formatting | bytes 524288
  (9 shorter events, 0.0 us)
Async XLA Ops:
  1.4 2.2 %copy-start = (bf16[1024,2048]{1,0:T(8,128)(2,1)S(1)}, bf16[1024,2048]{1,0:T(8,128)(2,1)}, u32[]{:S(2)}) copy-start(bf16[1024,2048]{1,0:T(8,128)(2,1)} %wo_hbm.1) | copy-start | bytes 12582916
  3.6 0.9 copy-start.3
  4.6 0.9 copy-start.4
  5.5 0.9 copy-start.5
  6.4 0.9 copy-start.6
  7.3 0.9 copy-start.7
  8.2 0.7 copy-start.8
  8.9 0.7 copy-start.9
  9.6 0.7 copy-start.10
  10.2 0.7 copy-start.11
  10.9 0.7 copy-start.12
  11.6 0.7 copy-start.13
  25.9 0.7 copy-start.1
  26.6 0.7 copy-start.2

commit v3 on v2

--- a/solution.py
+++ b/solution.py
@@ -192,16 +192,28 @@
         swap(d).wait_send()
 
 
+def fetched_kernel(count, *refs):
+    sources, rest, held, sem = refs[:count], refs[count:-count], refs[-count:-1], refs[-1]
+    plain = [i for i in range(count) if i != 9]
+    copies = [pltpu.make_async_copy(sources[i], b, sem.at[n]) for n, (i, b) in enumerate(zip(plain, held))]
+    for copy in copies:
+        copy.start()
+    for copy in copies:
+        copy.wait()
+    attention_kernel(*held[:9], sources[9], *held[9:], *rest)
+
+
 def attend(q, k, v, gate, score, added, logscale, strength_pre, gain, wo, skip, rescale, ids, shares, nz, lanes):
     heads, length = score.shape
     rows, width = skip.shape
     f32, bf = jnp.float32, jnp.bfloat16
     vm = pl.BlockSpec(memory_space=pltpu.VMEM)
     dma = pltpu.SemaphoreType.DMA
+    args = (q, k, v, gate, score, added, logscale, strength_pre, gain, wo, skip, rescale, ids, shares)
     return pl.pallas_call(
-        attention_kernel,
+        functools.partial(fetched_kernel, len(args)),
         out_shape=(jax.ShapeDtypeStruct((rows, width + lanes), bf), jax.ShapeDtypeStruct((rows, width), bf)),
-        in_specs=[vm] * 9 + [pl.BlockSpec(memory_space=pl.ANY)] + [vm] * 4,
+        in_specs=[pl.BlockSpec(memory_space=pl.ANY)] * len(args),
         out_specs=(vm, vm),
         scratch_shapes=[
             pltpu.VMEM((length, heads * HK), f32),
@@ -214,11 +226,12 @@
             pltpu.VMEM((nz, rows, heads * HK), bf),
             pltpu.VMEM(wo.shape, bf),
             dma, dma, dma, dma((nz,)), dma((nz,)),
+            *[pltpu.VMEM(a.shape, a.dtype) for i, a in enumerate(args) if i != 9], dma((len(args) - 1,)),
         ],
         compiler_params=pltpu.CompilerParams(
-            collective_id=5, has_side_effects=True, vmem_limit_bytes=48 * 1024 * 1024),
+            collective_id=5, has_side_effects=True, vmem_limit_bytes=VLIM),
         name="attend",
-    )(q, k, v, gate, score, added, logscale, strength_pre, gain, wo, skip, rescale, ids, shares)
+    )(*args)
 
 
 def experts_kernel(ny, nz, rows, width, experts, x_ref, merged_ref, wg_hbm, wu_hbm, wd_hbm, out_ref,

time: 116 us -> 107 us (0.922)
  local copies, waits for them, and re-layouts: 15.3 us -> 4.27 us
    unnamed x29 -> x1, local copies, waits for them, and re-layouts: 13.9 us -> 1.67 us
    pallas_call x1, Pallas kernels: 13.6 us -> 15.4 us  [attend(): pl.pallas_call(functools.partial(fetched_kernel, len(args)), out_shape=(j...]
where the time goes in v3:
time: 107 us
  Pallas kernels  102 us (95%)
  local copies, waits for them, and re-layouts  4.27 us (4%)
    pallas_call x1, Pallas kernels, run_experts(): pl.pallas_call(functools.partial(experts_kernel, ny, nz, rows, width, exp...  87 us
    pallas_call x1, Pallas kernels, attend(): pl.pallas_call(functools.partial(fetched_kernel, len(args)), out_shape=(j...  15.4 us

profile of v3, /device:TPU:10, one launch (start us, length us, event | category | flops | bytes accessed | tf_op | source)
XLA Modules:
  0.0 106.7 jit_solution(7509892243630234022)
XLA Ops:
  0.0 1.3 %copy.18.refs_6_ = f32[2,1]{1,0:T(2,128)} copy(f32[2,1]{0,1:T(1,128)} %bitcast.19) | data formatting | bytes 16 | tf_op jit(solution)/shard_map/broadcast_in_dim | solution.py:581
  1.3 1.3 %broadcast_in_dim.11.refs_11_ = bf16[1,2048]{1,0:T(2,128)(2,1)} reshape(bf16[2048]{0:T(1024)(128)(2,1)} %param.28) | data formatting | bytes 8192 | tf_op jit(solution)/shard_map/broadcast_in_dim | solution.py:586
  2.6 15.4 %attend.1 = (bf16[64,2176]{1,0:T(8,128)(2,1)}, bf16[64,2048]{1,0:T(8,128)(2,1)}) custom-call(bf16[256,256]{1,0:T(8,128)(2,1)} %refs_0_.1, bf16[256,256]{1,0:T(8,128)(2,1)} %refs_1_.1, bf16[256,256]{1,0:T(8,128)(2,1)} %refs_2_.1, bf16[256,256]{1,0:T(8,128)(2,1)} %refs_3_.1, f32[2,256]{1,0:T(2,128)} %bitcast.13, f32[2,256]{1,0:T(2,128)} %bitcast.14, ...), custom_call_target="tpu_custom_call" | custom-call | tf_op jit(solution)/shard_map/attend/pallas_call | solution.py:213
  18.1 87.0 %routed_experts.1 = bf16[64,2048]{1,0:T(8,128)(2,1)} custom-call(bf16[64,2176]{1,0:T(8,128)(2,1)} %get-tuple-element.7.x_ref, bf16[64,2048]{1,0:T(8,128)(2,1)} %get-tuple-element.8.merged_ref, bf16[2048,512]{1,0:T(8,128)(2,1)} %bitcast.10, bf16[2048,512]{1,0:T(8,128)(2,1)} %bitcast.11, bf16[512,2048]{1,0:T(8,128)(2,1)} %bitcast.12), custom_call_target="tpu_custom_call" | custom-call | tf_op jit(solution)/shard_map/routed_experts/pallas_call | solution.py:523
  105.0 1.7 %copy.20 = bf16[64,2048]{1,0:T(8,128)(2,1)} copy(bf16[64,2048]{1,0:T(8,128)(2,1)} %routed_experts.1) | data formatting | bytes 524288
